TPU v7x, 32 devices: a whole 2x2x4 slice. The times are simulated.
32 devices in a mesh: kv: 16 (over z, y, x), tp: 2 (over core).
Axes of the slice: x: 2, y: 2, z: 4, core: 2. Of those that a mesh axis runs over, the one named last changes fastest.
Arguments:
- tokens: bfloat16 [32, 4096], P(None, 'kv'), may hold values from -16 to 16
- mix_gain: bfloat16 [4096], P('kv'), may hold values from 0.099609375 to 1.8984375
- ffn_gain: bfloat16 [4096], P('kv'), may hold values from 0.099609375 to 1.8984375
- w_query: bfloat16 [4096, 2048], P('kv', 'tp'), may hold values from -0.09375 to 0.09375
- w_key: bfloat16 [4096, 2048], P('kv', 'tp'), may hold values from -0.09375 to 0.09375
- w_value: bfloat16 [4096, 4096], P('kv', 'tp'), may hold values from -0.09375 to 0.09375
- w_gate: bfloat16 [4096, 4096], P('kv', 'tp'), may hold values from -0.09375 to 0.09375
- w_decay: bfloat16 [4096, 2048], P('kv', 'tp'), may hold values from -0.375 to 0.375
- decay_bias: float32 [2048], P('tp'), may hold values from -7 to 4
- head_gain: bfloat16 [512], replicated, may hold values from 0.099609375 to 1.8984375
- w_output: bfloat16 [4096, 4096], P('tp', 'kv'), may hold values from -0.09375 to 0.09375
- w_ffgate: bfloat16 [4096, 11008], P('kv', 'tp'), may hold values from -0.09375 to 0.09375
- w_ffup: bfloat16 [4096, 11008], P('kv', 'tp'), may hold values from -0.09375 to 0.09375
- w_down: bfloat16 [11008, 4096], P('tp', 'kv'), may hold values from -0.0546875 to 0.0546875
- state: float32 [32, 8, 256, 512], P('kv', 'tp'), may hold values from -6 to 6
Outputs:
- mixed: bfloat16 [32, 4096], P(None, 'kv')
- new_state: float32 [32, 8, 256, 512], P('kv', 'tp')
All inputs are finite; a program needn't handle non-finite values.
Results may differ from a plain program's by a relative error of at most 0.015.
Values may be sent and summed in bfloat16 or wider, within the bound.
No kernel may reach another device: no remote copies, remote signals or barrier semaphores. Data moves between devices by JAX's collectives and lax.ppermute only.
A program may use at most 64 MiB of HBM per device.

v0:
```python
import jax
import jax.numpy as jnp
from jax import lax
from jax.sharding import PartitionSpec as P

epsilon = 1e-06


def local(
    tokens,
    mix_gain,
    ffn_gain,
    w_query,
    w_key,
    w_value,
    w_gate,
    w_decay,
    decay_bias,
    head_gain,
    w_output,
    w_ffgate,
    w_ffup,
    w_down,
    state,
):
    own_rows = state.shape[0]
    local_heads = state.shape[1]
    key_dim = state.shape[2]
    val_dim = state.shape[3]
    model_width = tokens.shape[1] * lax.axis_size("kv")
    row_offset = lax.axis_index("kv") * own_rows
    token_f32 = tokens.astype(jnp.float32)
    row_squares = jnp.sum(token_f32 * token_f32, axis=1)
    mix_in = (token_f32 * mix_gain.astype(jnp.float32)).astype(jnp.bfloat16)
    query_part = jnp.dot(mix_in, w_query, preferred_element_type=jnp.float32)
    key_part = jnp.dot(mix_in, w_key, preferred_element_type=jnp.float32)
    value_part = jnp.dot(mix_in, w_value, preferred_element_type=jnp.float32)
    gate_part = jnp.dot(mix_in, w_gate, preferred_element_type=jnp.float32)
    decay_part = jnp.dot(mix_in, w_decay, preferred_element_type=jnp.float32)
    square_total = lax.psum(row_squares, "kv")
    own_squares = lax.dynamic_slice_in_dim(square_total, row_offset, own_rows)
    query_sum, key_sum, value_sum, gate_sum, decay_sum = (
        lax.psum_scatter(query_part, "kv", scatter_dimension=0, tiled=True),
        lax.psum_scatter(key_part, "kv", scatter_dimension=0, tiled=True),
        lax.psum_scatter(value_part, "kv", scatter_dimension=0, tiled=True),
        lax.psum_scatter(gate_part, "kv", scatter_dimension=0, tiled=True),
        lax.psum_scatter(decay_part, "kv", scatter_dimension=0, tiled=True),
    )
    mix_rms = lax.rsqrt(own_squares / model_width + epsilon)[:, None]
    queries = (query_sum * mix_rms).reshape(own_rows, local_heads, key_dim) * key_dim ** (-0.5)
    key_rows = (key_sum * mix_rms).reshape(own_rows, local_heads, key_dim)
    value_rows = (value_sum * mix_rms).reshape(own_rows, local_heads, val_dim)
    gate_rows = (gate_sum * mix_rms).reshape(own_rows, local_heads, val_dim)
    decay_rows = (decay_sum * mix_rms + decay_bias).reshape(own_rows, local_heads, key_dim)
    log_decay = jax.nn.log_sigmoid(decay_rows) / 16.0
    new_state = (
        jnp.exp(log_decay)[..., None] * state + key_rows[..., :, None] * value_rows[..., None, :]
    )
    attended = jnp.einsum("bhk,bhkv->bhv", queries, new_state, precision=lax.Precision.HIGHEST)
    attended = attended * lax.rsqrt(
        jnp.sum(attended * attended, axis=2, keepdims=True) / val_dim + epsilon
    )
    head_out = (
        (attended * head_gain.astype(jnp.float32) * jax.nn.silu(gate_rows))
        .reshape(own_rows, local_heads * val_dim)
        .astype(jnp.bfloat16)
    )
    head_partial = jnp.dot(
        lax.all_gather(head_out, "kv", axis=0, tiled=True),
        w_output,
        preferred_element_type=jnp.float32,
    )
    attn_out = lax.psum(head_partial.astype(jnp.bfloat16), "tp").astype(jnp.float32)
    residual_mid = (token_f32 + attn_out).astype(jnp.bfloat16)
    mid_f32 = residual_mid.astype(jnp.float32)
    mid_squares = jnp.sum(mid_f32 * mid_f32, axis=1)
    ffn_in = (mid_f32 * ffn_gain.astype(jnp.float32)).astype(jnp.bfloat16)
    ffgate_part = jnp.dot(ffn_in, w_ffgate, preferred_element_type=jnp.float32)
    ffup_part = jnp.dot(ffn_in, w_ffup, preferred_element_type=jnp.float32)
    ffgate_sum, ffup_sum, square_sum = lax.psum((ffgate_part, ffup_part, mid_squares), "kv")
    ffn_rms = lax.rsqrt(square_sum / model_width + epsilon)[:, None]
    hidden = (jax.nn.silu(ffgate_sum * ffn_rms) * (ffup_sum * ffn_rms)).astype(jnp.bfloat16)
    down_part = jnp.dot(hidden, w_down, preferred_element_type=jnp.float32)
    ffn_out = lax.psum(down_part.astype(jnp.bfloat16), "tp").astype(jnp.float32)
    mixed = (mid_f32 + ffn_out).astype(jnp.bfloat16)
    return (mixed, new_state)


def solution(mesh):
    in_specs = (
        P(None, "kv"),
        P("kv"),
        P("kv"),
        P("kv", "tp"),
        P("kv", "tp"),
        P("kv", "tp"),
        P("kv", "tp"),
        P("kv", "tp"),
        P("tp"),
        P(),
        P("tp", "kv"),
        P("kv", "tp"),
        P("kv", "tp"),
        P("tp", "kv"),
        P("kv", "tp", None, None),
    )
    out_specs = (P(None, "kv"), P("kv", "tp", None, None))
    return jax.shard_map(local, mesh=mesh, in_specs=in_specs, out_specs=out_specs, check_vma=False)
```

profile of v0, /device:TPU:0, one launch (start us, length us, event | category | flops | bytes accessed | tf_op | source)
XLA Modules:
  0.0 317.6 jit_solution(6141432531111428591)
XLA Ops:
  7.2 0.0 copy-start
  7.2 0.0 copy-start.7
  7.2 0.0 copy-start.3
  7.2 0.0 copy-start.6
  7.2 0.0 copy-start.5
  7.2 0.0 copy-start.4
  7.2 0.0 all-reduce.12.cloned.1.call-start
  7.3 0.8 convert_element_type.49
  8.1 1.9 fusion.28
  10.0 1.9 fusion.26
  11.9 1.9 fusion.30
  13.9 2.2 fusion.24
  16.1 2.2 fusion.22
  18.3 0.0 all-reduce.12.cloned.1.call-update
  18.3 0.0 all-reduce.10.cloned.1.call-start
  18.4 0.0 copy-done.6
  18.4 0.0 copy-done.5
  18.5 0.0 copy-done.7
  18.5 0.6 dynamic-slice
  19.7 0.0 copy-done.3
  19.7 0.1 fusion.3
  19.8 43.7 %psum.42 = f32[32]{0:T(128)S(1)} all-reduce(f32[32]{0:T(128)S(1)} %fusion.3), channel_id=1, replica_groups=mesh['kv'=16,'tp'=2] {'kv'}, use_global_device_ids=true, to_apply=%region_2.0 | all-reduce | flops 32 | bytes 256 | tf_op jit(solution)/shard_map/psum | solution.py:40
  63.6 0.1 add_rsqrt_fusion.2
  63.6 70.8 %all-reduce.12.cloned.1.call-done = (f32[32,2048]{1,0:T(8,128)}, f32[32,1024]{1,0:T(8,128)}, f32[32,2048]{1,0:T(8,128)}, f32[32,1024]{1,0:T(8,128)}, f32[32,1024]{1,0:T(8,128)}) async-done(((f32[32,2048]{1,0:T(8,128)}, f32[32,1024]{1,0:T(8,128)}, f32[32,2048]{1,0:T(8,128)}, f32[32,1024]{1,0:T(8,128)}, f32[32,1024]{1,0:T(8,128)}), (f32[32,2048]{1,0:T(8,128)}, f32[32,1024]{1,0:T(8,128)}, ...) | async-done | bytes 917520
  134.4 0.0 copy-done.4
  134.4 0.9 fusion.20
  135.4 1.0 dynamic-slice_multiply_fusion.1
  136.4 2.6 multiply_add_fusion
  139.0 0.0 copy-start.1
  139.0 2.0 copy-done.1
  141.0 2.1 fusion.34
  143.1 0.1 fusion.9
  143.2 0.1 fusion.11
  143.3 39.5 %all-gather = bf16[16,2,2048]{2,1,0:T(2,128)(2,1)S(1)} all-gather(bf16[1,2,2048]{2,1,0:T(2,128)(2,1)S(1)} %reshape.47), channel_id=1, replica_groups=mesh['kv'=16,'tp'=2] {'kv'}, dimensions={0}, use_global_device_ids=true | all-gather | bytes 139264 | tf_op jit(solution)/shard_map/all_gather | solution.py:69
  182.9 0.1 reshape.48
  182.9 1.5 convolution_convert_fusion.1
  184.4 3.4 %psum.43 = bf16[32,256]{1,0:T(8,128)(2,1)S(1)} all-reduce(bf16[32,256]{1,0:T(8,128)(2,1)S(1)} %convolution_convert_fusion.1), channel_id=1, replica_groups=mesh['kv'=16,'tp'=2] {'tp'}, use_global_device_ids=true, to_apply=%region_8.9 | all-reduce | flops 8192 | bytes 32768 | tf_op jit(solution)/shard_map/psum | solution.py:73
  187.8 0.0 copy-start.2
  187.8 0.1 fusion.6
  187.9 0.0 copy-done
  187.9 1.5 fusion.12
  189.4 0.5 copy-done.2
  189.8 1.4 fusion.14
  191.3 0.0 all-reduce.10.cloned.1.call-update
  191.3 36.9 %psum.45 = f32[32]{0:T(128)S(1)} all-reduce(f32[32]{0:T(128)S(1)} %get-tuple-element.9), channel_id=1, replica_groups=mesh['kv'=16,'tp'=2] {'kv'}, use_global_device_ids=true, to_apply=%region_11.12 | all-reduce | flops 32 | bytes 256 | tf_op jit(solution)/shard_map/psum | solution.py:80
  228.2 75.7 %all-reduce.10.cloned.1.call-done = (f32[32,5504]{1,0:T(8,128)}, f32[32,5504]{1,0:T(8,128)}) async-done(((f32[32,5504]{1,0:T(8,128)}, f32[32,5504]{1,0:T(8,128)}), (f32[32,5504]{1,0:T(8,128)}, f32[32,5504]{1,0:T(8,128)})) %all-reduce.10.cloned.1.call-update) | async-done | bytes 1409040 | tf_op jit(solution)/shard_map/psum | solution.py:80
  303.9 2.8 convolution_convert_fusion
  306.8 3.4 %psum.47 = bf16[32,256]{1,0:T(8,128)(2,1)S(1)} all-reduce(bf16[32,256]{1,0:T(8,128)(2,1)S(1)} %convolution_convert_fusion), channel_id=1, replica_groups=mesh['kv'=16,'tp'=2] {'tp'}, use_global_device_ids=true, to_apply=%region_13.14 | all-reduce | flops 8192 | bytes 32768 | tf_op jit(solution)/shard_map/psum | solution.py:84
  310.1 0.6 fusion.7
  (11 shorter events, 0.2 us)
Async XLA Ops:
  7.2 180.7 %copy-start = (bf16[256,5504]{1,0:T(8,128)(2,1)S(1)}, bf16[256,5504]{1,0:T(8,128)(2,1)}, u32[]{:S(2)}) copy-start(bf16[256,5504]{1,0:T(8,128)(2,1)} %param.27) | copy-start | bytes 8454148
  7.2 11.3 %copy-start.7 = (u32[32]{0:T(128)S(1)}, u32[32]{0:T(128)}, u32[]{:S(2)}) copy-start(u32[32]{0:T(128)} %constant.41) | copy-start | bytes 388
  7.2 12.5 %copy-start.3 = (bf16[32,256]{1,0:T(8,128)(2,1)S(1)}, bf16[32,256]{1,0:T(8,128)(2,1)}, u32[]{:S(2)}) copy-start(bf16[32,256]{1,0:T(8,128)(2,1)} %param.15) | copy-start | bytes 49156
  7.2 11.2 %copy-start.6 = (bf16[256]{0:T(256)(128)(2,1)S(1)}, bf16[256]{0:T(256)(128)(2,1)}, u32[]{:S(2)}) copy-start(bf16[256]{0:T(256)(128)(2,1)} %param.17) | copy-start | bytes 1540
  7.2 11.2 %copy-start.5 = (bf16[512]{0:T(512)(128)(2,1)S(1)}, bf16[512]{0:T(512)(128)(2,1)}, u32[]{:S(2)}) copy-start(bf16[512]{0:T(512)(128)(2,1)} %param.24) | copy-start | bytes 3076
  7.2 127.2 %copy-start.4 = (f32[1024]{0:T(1024)S(1)}, f32[1024]{0:T(1024)}, u32[]{:S(2)}) copy-start(f32[1024]{0:T(1024)} %param.23) | copy-start | bytes 12292
  7.2 127.2 %all-reduce.12.cloned.1.call-start = ((), (), s32[]{:S(2)}) async-start(), calls=%async_computation.1 | async-start | bytes 1835008
  18.3 285.6 %all-reduce.10.cloned.1.call-start = ((), (), s32[]{:S(2)}) async-start(), calls=%async_computation | async-start | bytes 2818048 | tf_op jit(solution)/shard_map/psum | solution.py:80
  139.0 2.0 copy-start.1
  187.8 2.1 copy-start.2
Sparse Core Ops, SparseCore 0:
  18.5 115.9 all-reduce.11
  191.4 112.4 all-reduce.9
where the time goes:
time: 318 us
  waiting for transfers between devices  147 us (46%)
  blocking collectives  127 us (40%)
  matrix products  19.6 us (6%)
  between operations  14.9 us (5%)
  other arithmetic  6.37 us (2%)
  local copies, waits for them, and re-layouts  3.25 us (1%)
    psum x1, waiting for transfers between devices, local(): lax.psum((ffgate_part, ffup_part, mid_squares), 'kv')  75.7 us
    unnamed x3, waiting for transfers between devices  70.8 us
    psum x1, blocking collectives, local(): square_total = lax.psum(row_squares, 'kv')  43.7 us
    all_gather x1, blocking collectives, local(): lax.all_gather(head_out, 'kv', axis=0, tiled=True)  39.5 us
    psum x1, blocking collectives, local(): lax.psum((ffgate_part, ffup_part, mid_squares), 'kv')  36.9 us
  transfers between devices with their start and end apart: 2, of which 2 were waited for; matrix products, arithmetic and copies ran while one was open for 0% of the time, Pallas kernels for 0%

commit v1 on v0

--- a/solution.py
+++ b/solution.py
@@ -66,7 +66,9 @@
         .astype(jnp.bfloat16)
     )
     head_partial = jnp.dot(
-        lax.all_gather(head_out, "kv", axis=0, tiled=True),
+        jnp.concatenate(
+            lax.all_to_all(jnp.stack([head_out] * lax.axis_size("kv")), "kv", 0, 0), axis=0
+        ),
         w_output,
         preferred_element_type=jnp.float32,
     )

time: 318 us -> 293 us (0.921)
  blocking collectives: 127 us -> 88.8 us
  waiting for transfers between devices: 147 us -> 154 us
  starting transfers between devices: 0.08 us -> 4.84 us
    all_gather x1 -> x0, blocking collectives: 39.5 us -> none  [local(): lax.all_gather(head_out, 'kv', axis=0, tiled=True)]
    all_to_all x0 -> x1, waiting for transfers between devices: none -> 7.72 us  [local(): lax.all_to_all(jnp.stack([head_out] * lax.axis_size('kv')), 'kv', 0, 0)]
    all_to_all x0 -> x1, starting transfers between devices: none -> 4.76 us  [local(): lax.all_to_all(jnp.stack([head_out] * lax.axis_size('kv')), 'kv', 0, 0)]
  transfers between devices with their start and end apart: 2 -> 3, of which waited for: 2 -> 3; matrix products, arithmetic and copies ran while one was open for 0% -> 0% of each run, Pallas kernels for 0% -> 0%
where the time goes in v1:
time: 293 us; the launch traced here: 292 us
  waiting for transfers between devices  154 us (53%)
  blocking collectives  88.8 us (30%)
  matrix products  19.6 us (7%)
  between operations  14.9 us (5%)
  other arithmetic  6.37 us (2%)
  starting transfers between devices  4.84 us (2%)
  local copies, waits for them, and re-layouts  3.96 us (1%)
    psum x1, waiting for transfers between devices, local(): lax.psum((ffgate_part, ffup_part, mid_squares), 'kv')  75.1 us
    unnamed x3, waiting for transfers between devices  70.9 us
    psum x1, blocking collectives, local(): square_total = lax.psum(row_squares, 'kv')  43.9 us
    psum x1, blocking collectives, local(): lax.psum((ffgate_part, ffup_part, mid_squares), 'kv')  38.2 us
    all_to_all x1, waiting for transfers between devices, local(): lax.all_to_all(jnp.stack([head_out] * lax.axis_size('kv')), 'kv', 0, 0)  7.72 us
  transfers between devices with their start and end apart: 3, of which 3 were waited for; matrix products, arithmetic and copies ran while one was open for 0% of the time, Pallas kernels for 0%

profile of v1, /device:TPU:0, one launch (start us, length us, event | category | flops | bytes accessed | tf_op | source)
XLA Modules:
  0.0 292.1 jit_solution(14878677402918972135)
XLA Ops:
  7.2 0.0 copy-start
  7.2 0.0 copy-start.7
  7.2 0.0 copy-start.3
  7.2 0.0 copy-start.5
  7.2 0.0 copy-start.4
  7.2 0.0 all-reduce.12.cloned.1.call-start
  7.3 0.8 convert_element_type.51
  8.1 1.9 fusion.29
  10.0 1.9 fusion.27
  11.9 1.9 fusion.31
  13.8 2.2 fusion.25
  16.1 2.2 fusion.23
  18.3 0.0 all-reduce.12.cloned.1.call-update
  18.3 0.0 copy-done.5
  18.4 0.0 copy-done.7
  18.4 0.6 dynamic-slice
  19.6 0.0 copy-done.3
  19.6 0.1 fusion.3
  19.7 43.9 %psum.42 = f32[32]{0:T(128)S(1)} all-reduce(f32[32]{0:T(128)S(1)} %fusion.3), channel_id=1, replica_groups=mesh['kv'=16,'tp'=2] {'kv'}, use_global_device_ids=true, to_apply=%region_2.0 | all-reduce | flops 32 | bytes 256 | tf_op jit(solution)/shard_map/psum | solution.py:40
  63.6 0.1 add_rsqrt_fusion.2
  63.7 70.9 %all-reduce.12.cloned.1.call-done = (f32[32,2048]{1,0:T(8,128)}, f32[32,1024]{1,0:T(8,128)}, f32[32,2048]{1,0:T(8,128)}, f32[32,1024]{1,0:T(8,128)}, f32[32,1024]{1,0:T(8,128)}) async-done(((f32[32,2048]{1,0:T(8,128)}, f32[32,1024]{1,0:T(8,128)}, f32[32,2048]{1,0:T(8,128)}, f32[32,1024]{1,0:T(8,128)}, f32[32,1024]{1,0:T(8,128)}), (f32[32,2048]{1,0:T(8,128)}, f32[32,1024]{1,0:T(8,128)}, ...) | async-done | bytes 917520
  134.6 0.0 copy-done.4
  134.6 0.9 fusion.20
  135.5 1.0 dynamic-slice_multiply_fusion.1
  136.6 2.6 multiply_add_fusion
  139.2 0.0 copy-start.1
  139.2 2.0 copy-done.1
  141.2 0.0 copy-start.6
  141.2 2.1 fusion.35
  143.2 0.1 fusion.9
  143.4 0.1 fusion.22
  143.5 0.7 stack.2
  144.2 4.8 %all-to-all-start = ((bf16[16,2,2048]{2,1,0:T(2,128)(2,1)}), bf16[16,2,2048]{2,1,0:T(2,128)(2,1)S(1)}, u32[]{:S(2)}, u32[]{:S(2)}) async-start(bf16[16,2,2048]{2,1,0:T(2,128)(2,1)} %stack.2), calls=%async_computation | async-start | bytes 262144 | tf_op jit(solution)/shard_map/all_to_all | solution.py:70
  148.9 0.0 all-reduce.10.cloned.1.call-start
  149.0 0.0 copy-done.6
  149.0 7.7 %all-to-all-done = bf16[16,2,2048]{2,1,0:T(2,128)(2,1)S(1)} async-done(((bf16[16,2,2048]{2,1,0:T(2,128)(2,1)}), bf16[16,2,2048]{2,1,0:T(2,128)(2,1)S(1)}, u32[]{:S(2)}, u32[]{:S(2)}) %all-to-all-start) | async-done | bytes 131104 | tf_op jit(solution)/shard_map/all_to_all | solution.py:70
  156.7 0.1 reshape.53
  156.8 1.5 convolution_convert_fusion.1
  158.3 3.4 %psum.43 = bf16[32,256]{1,0:T(8,128)(2,1)S(1)} all-reduce(bf16[32,256]{1,0:T(8,128)(2,1)S(1)} %convolution_convert_fusion.1), channel_id=1, replica_groups=mesh['kv'=16,'tp'=2] {'tp'}, use_global_device_ids=true, to_apply=%region_8.9 | all-reduce | flops 8192 | bytes 32768 | tf_op jit(solution)/shard_map/psum | solution.py:75
  161.6 0.0 copy-start.2
  161.7 0.1 fusion.6
  161.8 0.0 copy-done
  161.8 1.5 fusion.12
  163.2 0.5 copy-done.2
  163.7 1.4 fusion.14
  165.2 0.0 all-reduce.10.cloned.1.call-update
  165.2 38.2 %psum.45 = f32[32]{0:T(128)S(1)} all-reduce(f32[32]{0:T(128)S(1)} %get-tuple-element.9), channel_id=1, replica_groups=mesh['kv'=16,'tp'=2] {'kv'}, use_global_device_ids=true, to_apply=%region_11.12 | all-reduce | flops 32 | bytes 256 | tf_op jit(solution)/shard_map/psum | solution.py:82
  203.4 75.1 %all-reduce.10.cloned.1.call-done = (f32[32,5504]{1,0:T(8,128)}, f32[32,5504]{1,0:T(8,128)}) async-done(((f32[32,5504]{1,0:T(8,128)}, f32[32,5504]{1,0:T(8,128)}), (f32[32,5504]{1,0:T(8,128)}, f32[32,5504]{1,0:T(8,128)})) %all-reduce.10.cloned.1.call-update) | async-done | bytes 1409040 | tf_op jit(solution)/shard_map/psum | solution.py:82
  278.4 2.8 convolution_convert_fusion
  281.3 3.4 %psum.47 = bf16[32,256]{1,0:T(8,128)(2,1)S(1)} all-reduce(bf16[32,256]{1,0:T(8,128)(2,1)S(1)} %convolution_convert_fusion), channel_id=1, replica_groups=mesh['kv'=16,'tp'=2] {'tp'}, use_global_device_ids=true, to_apply=%region_13.14 | all-reduce | flops 8192 | bytes 32768 | tf_op jit(solution)/shard_map/psum | solution.py:86
  284.6 0.6 fusion.7
  (11 shorter events, 0.2 us)
Async XLA Ops:
  7.2 154.6 %copy-start = (bf16[256,5504]{1,0:T(8,128)(2,1)S(1)}, bf16[256,5504]{1,0:T(8,128)(2,1)}, u32[]{:S(2)}) copy-start(bf16[256,5504]{1,0:T(8,128)(2,1)} %param.27) | copy-start | bytes 8454148
  7.2 11.2 %copy-start.7 = (u32[32]{0:T(128)S(1)}, u32[32]{0:T(128)}, u32[]{:S(2)}) copy-start(u32[32]{0:T(128)} %constant.41) | copy-start | bytes 388
  7.2 12.4 %copy-start.3 = (bf16[32,256]{1,0:T(8,128)(2,1)S(1)}, bf16[32,256]{1,0:T(8,128)(2,1)}, u32[]{:S(2)}) copy-start(bf16[32,256]{1,0:T(8,128)(2,1)} %param.15) | copy-start | bytes 49156
  7.2 11.1 %copy-start.5 = (bf16[512]{0:T(512)(128)(2,1)S(1)}, bf16[512]{0:T(512)(128)(2,1)}, u32[]{:S(2)}) copy-start(bf16[512]{0:T(512)(128)(2,1)} %param.24) | copy-start | bytes 3076
  7.2 127.4 %copy-start.4 = (f32[1024]{0:T(1024)S(1)}, f32[1024]{0:T(1024)}, u32[]{:S(2)}) copy-start(f32[1024]{0:T(1024)} %param.23) | copy-start | bytes 12292
  7.2 127.3 %all-reduce.12.cloned.1.call-start = ((), (), s32[]{:S(2)}) async-start(), calls=%async_computation.2 | async-start | bytes 1835008
  139.2 2.0 copy-start.1
  141.2 7.8 %copy-start.6 = (bf16[256]{0:T(256)(128)(2,1)S(1)}, bf16[256]{0:T(256)(128)(2,1)}, u32[]{:S(2)}) copy-start(bf16[256]{0:T(256)(128)(2,1)} %param.17) | copy-start | bytes 1540
  144.2 12.6 %all-to-all-start = ((bf16[16,2,2048]{2,1,0:T(2,128)(2,1)}), bf16[16,2,2048]{2,1,0:T(2,128)(2,1)S(1)}, u32[]{:S(2)}, u32[]{:S(2)}) async-start(bf16[16,2,2048]{2,1,0:T(2,128)(2,1)} %stack.2), calls=%async_computation | async-start | bytes 262144 | tf_op jit(solution)/shard_map/all_to_all | solution.py:70
  148.9 129.5 %all-reduce.10.cloned.1.call-start = ((), (), s32[]{:S(2)}) async-start(), calls=%async_computation.1 | async-start | bytes 2818048 | tf_op jit(solution)/shard_map/psum | solution.py:82
  161.6 2.1 copy-start.2
Sparse Core Ops, SparseCore 0:
  18.5 116.0 all-reduce.11
  165.3 113.0 all-reduce.9
